TPU v7x, 32 devices: a whole 2x2x4 slice. The times are simulated.
32 devices in a mesh: sp: 16 (over z, y, x), tp: 2 (over core).
Axes of the slice: x: 2, y: 2, z: 4, core: 2. Of those that a mesh axis runs over, the one named last changes fastest.
Arguments:
- tokens: bfloat16 [4096, 4096], P('sp', 'tp'), may hold values from -480 to 480
- gain: float32 [4096], P('tp'), may hold values from 0.1 to 1.9
- q_att: bfloat16 [4096, 2048], P('sp', 'tp'), may hold values from -2.90625 to 2.90625
- k_att: bfloat16 [4096, 1024], P('sp', 'tp'), may hold values from -0.09375 to 0.09375
- v_att: bfloat16 [4096, 1024], P('sp', 'tp'), may hold values from -0.75 to 0.75
- q_ret: bfloat16 [4096, 1024], P('sp', 'tp'), may hold values from -0.09375 to 0.09375
- k_ret: bfloat16 [4096, 1024], P('sp', 'tp'), may hold values from -0.09375 to 0.09375
- v_ret: bfloat16 [4096, 1024], P('sp', 'tp'), may hold values from -0.09375 to 0.09375
- out_att: bfloat16 [2048, 4096], P('tp', 'sp'), may hold values from -0.109375 to 0.109375
- out_ret: bfloat16 [1024, 4096], P('tp', 'sp'), may hold values from -0.109375 to 0.109375
- sink: float32 [16], P('tp'), may hold values from 3 to 7
- decay_log: float32 [8, 4096], P('tp', 'sp'), may hold values from -2.125 to 0
Outputs:
- mixed: bfloat16 [4096, 4096], P(('sp', 'tp'))
- log_weight: float32 [16, 4096], P('tp', 'sp')
All inputs are finite; a program needn't handle non-finite values.
Results may differ from a plain program's by a relative error of at most 0.017.
Values may be sent and summed in bfloat16 or wider, within the bound.
A program may use at most 128 MiB of HBM per device.

v0:
```python
import jax
import jax.numpy as jnp
from jax import lax
from jax.sharding import PartitionSpec as P

D = 4096
HEAD_DIM = 128
SPAN_RADIUS = 128


def with_halo(shard, sides, width):
    for axis, dim in sides:
        peers, length = (lax.axis_size(axis), shard.shape[dim])
        up = [(i, (i + 1) % peers) for i in range(peers - 1)]
        down = [(j, i) for i, j in up]
        last = lax.slice_in_dim(shard, length - width, length, axis=dim)
        initial = lax.slice_in_dim(shard, 0, width, axis=dim)
        before = lax.ppermute(last, axis, up)
        after = lax.ppermute(initial, axis, down)
        shard = jnp.concatenate([before, shard, after], axis=dim)
    return shard


def entering(shard, axis, combine, identity, reverse):
    peers, index = (lax.axis_size(axis), lax.axis_index(axis))
    everything = jax.tree.map(
        lambda part, kind: lax.all_gather(part.astype(kind), axis),
        shard,
        (jnp.bfloat16, jnp.bfloat16),
    )
    start = jax.tree.map(
        lambda part, zero: jnp.broadcast_to(jnp.asarray(zero, part.dtype), part.shape),
        shard,
        identity,
    )

    def turn(k, before):
        at = peers - 1 - k if reverse else k
        reached = at > index if reverse else at < index
        new = combine(
            before, jax.tree.map(lambda part, own: part[at].astype(own.dtype), everything, shard)
        )
        return jax.tree.map(lambda a, b: jnp.where(reached, a, b), new, before)

    return lax.fori_loop(0, peers, turn, start)


def rotate(values, angles):
    half = values.shape[-1] // 2
    first = values[..., :half]
    second = values[..., half:]
    cosine = jnp.cos(angles)[:, None, :]
    sine = jnp.sin(angles)[:, None, :]
    return jnp.concatenate(
        [first * cosine - second * sine, second * cosine + first * sine], axis=-1
    )


def fold_with(weights, piece):
    return tuple((jnp.dot(piece, weight, preferred_element_type=jnp.float32) for weight in weights))


def chain(earlier, later):
    return (earlier[0] * later[0], later[0][:, None, None] * earlier[1] + later[1])


def shards(
    tokens, gain, q_att, k_att, v_att, q_ret, k_ret, v_ret, out_att, out_ret, sink, decay_log
):
    tok_rows = tokens.shape[0]
    att_local = sink.shape[0]
    nearby_memory = k_att.shape[1] // HEAD_DIM
    ret_local = q_ret.shape[1] // HEAD_DIM
    group = att_local // nearby_memory
    total_rows = tok_rows * lax.axis_size("sp")
    offset = lax.axis_index("sp") * tok_rows
    highest = lax.Precision.HIGHEST
    widened = tokens.astype(jnp.float32)
    squares = lax.psum(jnp.sum(widened * widened, axis=1), "tp")
    inverse = lax.rsqrt(squares / D + 1e-06)[:, None]
    scaled = (widened * gain).astype(jnp.bfloat16)
    wide_qa, wide_ka, wide_va, wide_qr, wide_kr, wide_vr = (
        lax.all_gather(q_att, "sp", axis=0, tiled=True),
        lax.all_gather(k_att, "sp", axis=0, tiled=True),
        lax.all_gather(v_att, "sp", axis=0, tiled=True),
        lax.all_gather(q_ret, "sp", axis=0, tiled=True),
        lax.all_gather(k_ret, "sp", axis=0, tiled=True),
        lax.all_gather(v_ret, "sp", axis=0, tiled=True),
    )
    every_weight = (wide_qa, wide_ka, wide_va, wide_qr, wide_kr, wide_vr)
    proj_qa, proj_ka, proj_va, proj_qr, proj_kr, proj_vr = fold_with(
        every_weight, lax.all_gather(scaled, "tp", axis=1, tiled=True)
    )
    positions = (offset + jnp.arange(tok_rows, dtype=jnp.int32)).astype(jnp.float32)
    freqs = 10000.0 ** (-jnp.arange(0, HEAD_DIM, 2).astype(jnp.float32) / HEAD_DIM)
    angles = positions[:, None] * freqs[None, :]
    att_query = rotate((proj_qa * inverse).reshape(tok_rows, att_local, HEAD_DIM), angles).astype(
        jnp.bfloat16
    )
    att_key = rotate((proj_ka * inverse).reshape(tok_rows, nearby_memory, HEAD_DIM), angles).astype(
        jnp.bfloat16
    )
    att_value = (proj_va * inverse).astype(jnp.bfloat16).reshape(tok_rows, nearby_memory, HEAD_DIM)
    stacked = jnp.stack([att_key, att_value])
    widened_pair = with_halo(stacked, (("sp", 1),), SPAN_RADIUS)
    block_rows = min(tok_rows, 512)
    sink_logit = sink.reshape(nearby_memory, group)
    grouped_query = att_query.reshape(tok_rows, nearby_memory, group, HEAD_DIM)

    def attend_block(index):
        begin = index * block_rows
        block_keys = widened_pair[0]
        block_values = widened_pair[1]
        scores = jnp.einsum(
            "qhgd,khd->hgqk", grouped_query, block_keys, preferred_element_type=jnp.float32
        ) * HEAD_DIM ** (-0.5)
        query_pos = offset + begin + jnp.arange(block_rows, dtype=jnp.int32)
        key_pos = (
            offset + begin - SPAN_RADIUS + jnp.arange(block_rows + 2 * SPAN_RADIUS, dtype=jnp.int32)
        )
        spacing = key_pos[None, :] - query_pos[:, None]
        valid = (
            (jnp.abs(spacing) <= SPAN_RADIUS)
            & (key_pos >= 0)[None, :]
            & (key_pos < total_rows)[None, :]
        )
        masked = jnp.where(valid, scores, -jnp.inf)
        top = jnp.maximum(jnp.max(masked, axis=-1), sink_logit[:, :, None])
        expo = jnp.exp(masked - top[..., None])
        total = jnp.sum(expo, axis=-1) + jnp.exp(sink_logit[:, :, None] - top)
        logs = top + jnp.log(total)
        probs = (expo / total[..., None]).astype(jnp.bfloat16)
        result = jnp.einsum(
            "hgqk,khd->qhgd", probs, block_values, preferred_element_type=jnp.float32
        ).astype(jnp.bfloat16)
        return (
            result.reshape(block_rows, att_local * HEAD_DIM),
            logs.reshape(att_local, block_rows),
        )

    att_blocks, log_blocks = lax.map(
        attend_block, jnp.arange(tok_rows // block_rows, dtype=jnp.int32)
    )
    att_out = att_blocks.reshape(tok_rows, att_local * HEAD_DIM)
    log_weight = jnp.moveaxis(log_blocks, 0, 1).reshape(att_local, tok_rows)
    ret_query = (proj_qr * inverse).astype(jnp.bfloat16).reshape(tok_rows, ret_local, HEAD_DIM)
    ret_key = (
        (proj_kr * (inverse * HEAD_DIM ** (-0.5)))
        .astype(jnp.bfloat16)
        .reshape(tok_rows, ret_local, HEAD_DIM)
    )
    ret_value = (proj_vr * inverse).astype(jnp.bfloat16).reshape(tok_rows, ret_local, HEAD_DIM)
    cumul = jnp.cumsum(decay_log, axis=1)
    last = cumul[:, -1]
    query_f = ret_query.astype(jnp.float32)
    key_f = ret_key.astype(jnp.float32)
    value_f = ret_value.astype(jnp.float32)
    ret_scores = jnp.einsum("qhd,khd->hqk", ret_query, ret_key, preferred_element_type=jnp.float32)
    decay_weights = jnp.exp(-jnp.abs(cumul[:, :, None] - cumul[:, None, :]))
    inner = jnp.einsum("hqk,khd->qhd", ret_scores * decay_weights, value_f, precision=highest)
    trailing = jnp.exp(last[:, None] - cumul)
    leading = jnp.exp(cumul)
    forward_state = jnp.einsum("hk,khd,khe->hde", trailing, key_f, value_f, precision=highest)
    backward_state = jnp.einsum("hk,khd,khe->hde", leading, key_f, value_f, precision=highest)
    decay_total = jnp.exp(last)
    identity = (jnp.ones_like(decay_total), jnp.zeros_like(forward_state))
    from_before = entering((decay_total, forward_state), "sp", chain, identity, False)[1]
    from_after = entering((decay_total, backward_state), "sp", chain, identity, True)[1]
    carried = leading.T[:, :, None] * jnp.einsum(
        "qhd,hde->qhe", query_f, from_before, precision=highest
    )
    carried = carried + trailing.T[:, :, None] * jnp.einsum(
        "qhd,hde->qhe", query_f, from_after, precision=highest
    )
    blended_output = inner + carried
    middle_point = blended_output - jnp.mean(blended_output, axis=-1, keepdims=True)
    normed = middle_point * lax.rsqrt(
        jnp.mean(middle_point * middle_point, axis=-1, keepdims=True) + 1e-06
    )
    ret_out = normed.astype(jnp.bfloat16).reshape(tok_rows, ret_local * HEAD_DIM)
    wide_out_att, wide_out_ret = (
        lax.all_gather(out_att, "sp", axis=1, tiled=True),
        lax.all_gather(out_ret, "sp", axis=1, tiled=True),
    )
    mixed = lax.psum_scatter(
        (
            jnp.dot(att_out, wide_out_att, preferred_element_type=jnp.float32)
            + jnp.dot(ret_out, wide_out_ret, preferred_element_type=jnp.float32)
        ).astype(jnp.bfloat16),
        "tp",
        scatter_dimension=0,
        tiled=True,
    )
    return (mixed, log_weight)


def solution(mesh):
    return jax.shard_map(
        shards,
        mesh=mesh,
        in_specs=(
            P("sp", "tp"),
            P("tp"),
            P("sp", "tp"),
            P("sp", "tp"),
            P("sp", "tp"),
            P("sp", "tp"),
            P("sp", "tp"),
            P("sp", "tp"),
            P("tp", "sp"),
            P("tp", "sp"),
            P("tp"),
            P("tp", "sp"),
        ),
        out_specs=(P(("sp", "tp"), None), P("tp", "sp")),
        check_vma=False,
    )
```

profile of v0, /device:TPU:0, one launch (start us, length us, event | category | flops | bytes accessed | tf_op | source)
XLA Modules:
  0.0 895.8 jit_solution(7735527587921231865)
XLA Ops:
  7.2 2.5 fusion.6
  13.0 1.2 reduce-window.6
  14.8 2.6 psum.7
  17.5 5.9 all-gather.15.cloned.1.call-done
  23.4 79.6 %all-gather.29.cloned.1.call-done = bf16[4096,512]{1,0:T(8,128)(2,1)} async-done(((bf16[256,512]{1,0:T(8,128)(2,1)}), bf16[4096,512]{1,0:T(8,128)(2,1)}) %all-gather.29.cloned.1.call-update) | async-done | bytes 4194320 | tf_op jit(solution)/shard_map/all_gather | solution.py:87
  103.0 4.1 fusion.17
  107.2 72.8 %all-gather.25.cloned.1.call-done = bf16[4096,512]{1,0:T(8,128)(2,1)} async-done(((bf16[256,512]{1,0:T(8,128)(2,1)}), bf16[4096,512]{1,0:T(8,128)(2,1)}) %all-gather.25.cloned.1.call-update) | async-done | bytes 4194320 | tf_op jit(solution)/shard_map/all_gather | solution.py:88
  180.0 4.1 fusion.19
  184.1 1.1 convolution_convert_fusion
  185.3 1.0 convolution_convert_fusion.1
  190.1 39.8 %all-reduce = bf16[64]{0:T(256)(128)(2,1)S(1)} all-reduce(bf16[64]{0:T(256)(128)(2,1)S(1)} %dynamic-update-slice), channel_id=2, replica_groups=mesh['sp'=16,'tp'=2] {'sp'}, use_global_device_ids=true, to_apply=%add | all-reduce | flops 64 | bytes 256
  231.4 25.6 %all-gather.17.cloned.1.call-done = bf16[4096,512]{1,0:T(8,128)(2,1)} async-done(((bf16[256,512]{1,0:T(8,128)(2,1)}), bf16[4096,512]{1,0:T(8,128)(2,1)}) %all-gather.17.cloned.1.call-update) | async-done | bytes 4194320 | tf_op jit(solution)/shard_map/all_gather | solution.py:84
  257.1 4.1 convolution_multiply_fusion.6
  261.7 72.2 %all-gather.19.cloned.1.call-done = bf16[4096,512]{1,0:T(8,128)(2,1)} async-done(((bf16[256,512]{1,0:T(8,128)(2,1)}), bf16[4096,512]{1,0:T(8,128)(2,1)}) %all-gather.19.cloned.1.call-update) | async-done | bytes 4194320 | tf_op jit(solution)/shard_map/all_gather | solution.py:85
  333.9 4.1 fusion.14
  339.2 3.4 collective-permute-start
  342.6 1.3 collective-permute-start.1
  343.9 70.2 %all-gather.27.cloned.1.call-done = bf16[4096,512]{1,0:T(8,128)(2,1)} async-done(((bf16[256,512]{1,0:T(8,128)(2,1)}), bf16[4096,512]{1,0:T(8,128)(2,1)}) %all-gather.27.cloned.1.call-update) | async-done | bytes 4194320 | tf_op jit(solution)/shard_map/all_gather | solution.py:86
  414.0 4.1 fusion.18
  418.2 1.3 convolution_multiply_fusion
  419.4 1.1 pad_maximum_fusion
  420.6 55.2 %all-gather.35.cloned.1.call-done = bf16[64,128,128]{2,1,0:T(8,128)(2,1)} async-done(((bf16[4,128,128]{2,1,0:T(8,128)(2,1)}), bf16[64,128,128]{2,1,0:T(8,128)(2,1)}) %all-gather.35.cloned.1.call-update) | async-done | bytes 2097168 | tf_op jit(solution)/shard_map/all_gather | solution.py:27
  475.8 27.7 %while.36 = (s32[]{:T(128)}, f32[4,128,128]{2,1,0:T(8,128)S(1)}, s32[]{:T(128)}, bf16[16,4]{1,0:T(8,128)(2,1)}, bf16[16,4,128,128]{3,2,1,0:T(8,128)(2,1)}, /*index=5*/s32[]{:T(128)}, s32[]{:T(128)}, s32[]{:T(128)}, s32[]{:T(128)}) while((s32[]{:T(128)}, f32[4,128,128]{2,1,0:T(8,128)S(1)}, s32[]{:T(128)}, bf16[16,4]{1,0:T(8,128)(2,1)}, ...), condition=%wide.region_9.10_spmd.clone, body=%wide.region_8.9_spmd.clone.sunk | while | flops 327692 | bytes 655567 | solution.py:45
  476.6 1.0 fusion.75
  478.3 1.0 fusion.75
  480.0 1.0 fusion.75
  481.8 1.0 fusion.75
  483.5 1.0 fusion.75
  485.2 1.0 fusion.75
  486.9 1.0 fusion.75
  492.1 1.0 fusion.75
  493.8 1.0 fusion.75
  503.5 34.4 %all-gather.33.cloned.1.call-done = bf16[64,128,128]{2,1,0:T(8,128)(2,1)} async-done(((bf16[4,128,128]{2,1,0:T(8,128)(2,1)}), bf16[64,128,128]{2,1,0:T(8,128)(2,1)}) %all-gather.33.cloned.1.call-update) | async-done | bytes 2097168 | tf_op jit(solution)/shard_map/all_gather | solution.py:27
  537.9 27.5 %while.35 = (s32[]{:T(128)}, f32[4,128,128]{2,1,0:T(8,128)S(1)}, s32[]{:T(128)}, bf16[16,4]{1,0:T(8,128)(2,1)}, bf16[16,4,128,128]{3,2,1,0:T(8,128)(2,1)}, /*index=5*/s32[]{:T(128)}, s32[]{:T(128)}) while((s32[]{:T(128)}, f32[4,128,128]{2,1,0:T(8,128)S(1)}, s32[]{:T(128)}, bf16[16,4]{1,0:T(8,128)(2,1)}, ...), condition=%wide.region_7.8_spmd.clone, body=%wide.region_6.7_spmd.clone.sunk | while | flops 327688 | bytes 655505 | solution.py:45
  547.2 1.0 fusion.74
  548.9 1.0 fusion.74
  555.8 1.0 fusion.74
  559.2 1.0 fusion.74
  560.9 1.0 fusion.74
  567.2 84.6 %all-gather.21.cloned.1.call-done = bf16[4096,1024]{1,0:T(8,128)(2,1)} async-done(((bf16[256,1024]{1,0:T(8,128)(2,1)}), bf16[4096,1024]{1,0:T(8,128)(2,1)}) %all-gather.21.cloned.1.call-update) | async-done | bytes 8388624 | tf_op jit(solution)/shard_map/all_gather | solution.py:83
  651.8 6.3 fusion.8
  659.0 1.0 fusion.4
  661.1 1.3 fusion.9
  662.4 124.7 %all-gather.23.cloned.1.call-done = bf16[1024,4096]{1,0:T(8,128)(2,1)} async-done(((bf16[1024,256]{1,0:T(8,128)(2,1)}), bf16[1024,4096]{1,0:T(8,128)(2,1)}) %all-gather.23.cloned.1.call-update) | async-done | bytes 8388624 | tf_op jit(solution)/shard_map/all_gather | solution.py:182
  787.1 7.8 fusion.51
  794.8 80.0 %all-gather.31.cloned.1.call-done = bf16[512,4096]{1,0:T(8,128)(2,1)} async-done(((bf16[512,256]{1,0:T(8,128)(2,1)}), bf16[512,4096]{1,0:T(8,128)(2,1)}) %all-gather.31.cloned.1.call-update) | async-done | bytes 4194320 | tf_op jit(solution)/shard_map/all_gather | solution.py:183
  874.8 6.1 fusion.2
  881.6 7.4 reduce-scatter.2.cloned.1.call-done
  (146 shorter events, 55.0 us)
Async XLA Ops:
  7.2 5.9 copy-start.3
  7.2 16.3 %all-gather.15.cloned.1.call-start = ((), (), s32[]{:S(2)}) async-start(), calls=%async_computation.1 | async-start | bytes 3145728 | tf_op jit(solution)/shard_map/all_gather | solution.py:92
  9.7 93.3 %all-gather.29.cloned.1.call-start = ((), (), s32[]{:S(2)}) async-start(), calls=%async_computation.8 | async-start | bytes 4456448 | tf_op jit(solution)/shard_map/all_gather | solution.py:87
  10.5 169.5 %all-gather.25.cloned.1.call-start = ((), (), s32[]{:S(2)}) async-start(), calls=%async_computation.6 | async-start | bytes 4456448 | tf_op jit(solution)/shard_map/all_gather | solution.py:88
  11.2 245.8 %all-gather.17.cloned.1.call-start = ((), (), s32[]{:S(2)}) async-start(), calls=%async_computation.2 | async-start | bytes 4456448 | tf_op jit(solution)/shard_map/all_gather | solution.py:84
  11.8 322.1 %all-gather.19.cloned.1.call-start = ((), (), s32[]{:S(2)}) async-start(), calls=%async_computation.3 | async-start | bytes 4456448 | tf_op jit(solution)/shard_map/all_gather | solution.py:85
  12.4 401.6 %all-gather.27.cloned.1.call-start = ((), (), s32[]{:S(2)}) async-start(), calls=%async_computation.7 | async-start | bytes 4456448 | tf_op jit(solution)/shard_map/all_gather | solution.py:86
  13.0 462.8 %all-gather.35.cloned.1.call-start = ((), (), s32[]{:S(2)}) async-start(), calls=%async_computation.12 | async-start | bytes 2228224 | tf_op jit(solution)/shard_map/all_gather | solution.py:27
  17.5 316.5 %copy-start.6 = (f32[256]{0:T(256)}, f32[256]{0:T(256)S(1)}, u32[]{:S(2)}) copy-start(f32[256]{0:T(256)S(1)} %get-tuple-element.322) | copy-start | bytes 3076
  107.2 78.0 %copy-start.1 = (bf16[256,512]{0,1:T(8,128)(2,1)}, bf16[256,512]{0,1:T(8,128)(2,1)S(1)}, u32[]{:S(2)}) copy-start(bf16[256,512]{0,1:T(8,128)(2,1)S(1)} %copy.80) | copy-start | bytes 786436
  180.0 8.5 copy-start.4
  180.0 8.6 copy-start.8
  185.2 352.7 %all-gather.33.cloned.1.call-start = ((), (), s32[]{:S(2)}) async-start(), calls=%async_computation.11 | async-start | bytes 2228224 | tf_op jit(solution)/shard_map/all_gather | solution.py:27
  186.3 465.5 %all-gather.21.cloned.1.call-start = ((), (), s32[]{:S(2)}) async-start(), calls=%async_computation.4 | async-start | bytes 8912896 | tf_op jit(solution)/shard_map/all_gather | solution.py:83
  187.1 600.0 %all-gather.23.cloned.1.call-start = ((), (), s32[]{:S(2)}) async-start(), calls=%async_computation.5 | async-start | bytes 8912896 | tf_op jit(solution)/shard_map/all_gather | solution.py:182
  187.6 687.1 %all-gather.31.cloned.1.call-start = ((), (), s32[]{:S(2)}) async-start(), calls=%async_computation.9 | async-start | bytes 4456448 | tf_op jit(solution)/shard_map/all_gather | solution.py:183
  188.4 700.6 %reduce-scatter.2.cloned.1.call-start = ((), (), s32[]{:S(2)}) async-start(), calls=%async_computation.10 | async-start | bytes 3145728 | tf_op jit(solution)/shard_map/reduce_scatter | solution.py:185
  338.4 79.7 %copy-start.2 = (bf16[256,512]{0,1:T(8,128)(2,1)S(1)}, bf16[256,512]{0,1:T(8,128)(2,1)}, u32[]{:S(2)}) copy-start(bf16[256,512]{0,1:T(8,128)(2,1)} %copy-done.1) | copy-start | bytes 786436
  339.2 80.2 %collective-permute-start = (bf16[2,128,4,128]{3,1,2,0:T(8,128)(2,1)}, bf16[2,128,4,128]{3,1,2,0:T(8,128)(2,1)S(1)}, u32[]{:S(2)}, u32[]{:S(2)}) collective-permute-start(bf16[2,128,4,128]{3,1,2,0:T(8,128)(2,1)} %get-tuple-element.313), channel_id=1, source_target_pairs={{0,2},{2,4},{4,6},{6,8},{8,10},{10,12},{12,14},{14,16},{16,18},{18... | collective-permute-start | bytes 786440 | tf_op jit(solution)/shard_map/ppermute | solution.py:18
  342.6 76.9 %collective-permute-start.1 = (bf16[2,128,4,128]{3,1,2,0:T(8,128)(2,1)S(1)}, bf16[2,128,4,128]{3,1,2,0:T(8,128)(2,1)}, u32[]{:S(2)}, u32[]{:S(2)}) collective-permute-start(bf16[2,128,4,128]{3,1,2,0:T(8,128)(2,1)S(1)} %get-tuple-element.314), channel_id=1, source_target_pairs={{2,0},{4,2},{6,4},{8,6},{10,8},{12,10},{14,12},{16,14},{18,16},{20... | collective-permute-start | bytes 786440 | tf_op jit(solution)/shard_map/ppermute | solution.py:19
  475.8 90.5 %copy-start = (f32[4,256,256]{2,1,0:T(8,128)S(1)}, f32[4,256,256]{2,1,0:T(8,128)}, u32[]{:S(2)}) copy-start(f32[4,256,256]{2,1,0:T(8,128)} %convolution_multiply_fusion) | copy-start | bytes 3145732
  565.4 86.4 %copy-start.7 = (f32[256]{0:T(256)S(1)}, f32[256]{0:T(256)}, u32[]{:S(2)}) copy-start(f32[256]{0:T(256)} %copy-done.6) | copy-start | bytes 3076
  874.8 6.1 copy-start.5
Sparse Core Ops, SparseCore 0:
  10.1 13.2 all-gather.14
  26.2 76.7 all-gather.28
  105.8 74.1 all-gather.24
  182.6 74.4 all-gather.16
  259.7 74.1 all-gather.18
  336.5 77.4 all-gather.26
  416.8 58.9 all-gather.34
  478.6 59.2 all-gather.32
  540.7 111.0 all-gather.20
  654.4 132.6 all-gather.22
  789.8 84.9 all-gather.30
  881.0 7.9 reduce-scatter.1
where the time goes:
time: 897 us; the launch traced here: 896 us
  waiting for transfers between devices  717 us (80%)
  other arithmetic  63.1 us (7%)
  matrix products  47.8 us (5%)
  blocking collectives  42.4 us (5%)
  between operations  15.3 us (2%)
    all_gather x1, waiting for transfers between devices, shards(): lax.all_gather(out_att, 'sp', axis=1, tiled=True)  125 us
    all_gather x2, waiting for transfers between devices, entering(): lax.all_gather(part.astype(kind), axis)  89.6 us
    all_gather x1, waiting for transfers between devices, shards(): lax.all_gather(q_att, 'sp', axis=0, tiled=True)  84.6 us
    all_gather x1, waiting for transfers between devices, shards(): lax.all_gather(out_ret, 'sp', axis=1, tiled=True)  80 us
    all_gather x1, waiting for transfers between devices, shards(): lax.all_gather(k_ret, 'sp', axis=0, tiled=True)  79.6 us
    all_gather x1, waiting for transfers between devices, shards(): lax.all_gather(v_ret, 'sp', axis=0, tiled=True)  72.8 us
    all_gather x1, waiting for transfers between devices, shards(): lax.all_gather(v_att, 'sp', axis=0, tiled=True)  72.2 us
    all_gather x1, waiting for transfers between devices, shards(): lax.all_gather(q_ret, 'sp', axis=0, tiled=True)  70.2 us
  transfers between devices with their start and end apart: 14, of which 12 were waited for; matrix products, arithmetic and copies ran while one was open for 12% of the time, Pallas kernels for 0%

commit v1 on v0

--- a/solution.py
+++ b/solution.py
@@ -6,6 +6,12 @@
 D = 4096
 HEAD_DIM = 128
 SPAN_RADIUS = 128
+
+
+def all_parts(value, axis, along):
+    parts = lax.all_gather(value, axis, axis=0, tiled=False)
+    full = jnp.concatenate(parts, axis=along)
+    return full
 
 
 def with_halo(shard, sides, width):
@@ -180,7 +186,7 @@
     ret_out = normed.astype(jnp.bfloat16).reshape(tok_rows, ret_local * HEAD_DIM)
     wide_out_att, wide_out_ret = (
         lax.all_gather(out_att, "sp", axis=1, tiled=True),
-        lax.all_gather(out_ret, "sp", axis=1, tiled=True),
+        all_parts(out_ret, "sp", 1),
     )
     mixed = lax.psum_scatter(
         (

time: 897 us -> 889 us (level)
  waiting for transfers between devices: 717 us -> 706 us
    all_gather x1, waiting for transfers between devices: 80 us -> 69.9 us  [all_parts(): parts = lax.all_gather(value, axis, axis=0, tiled=False)]
where the time goes in v1:
time: 889 us; the launch traced here: 887 us
  waiting for transfers between devices  706 us (79%)
  other arithmetic  62.1 us (7%)
  matrix products  45 us (5%)
  blocking collectives  42.4 us (5%)
  between operations  15.3 us (2%)
  local copies, waits for them, and re-layouts  9.69 us (1%)
    all_gather x1, waiting for transfers between devices, shards(): lax.all_gather(out_att, 'sp', axis=1, tiled=True)  125 us
    all_gather x2, waiting for transfers between devices, entering(): lax.all_gather(part.astype(kind), axis)  89.2 us
    all_gather x1, waiting for transfers between devices, shards(): lax.all_gather(q_att, 'sp', axis=0, tiled=True)  82.9 us
    all_gather x1, waiting for transfers between devices, shards(): lax.all_gather(k_ret, 'sp', axis=0, tiled=True)  79.6 us
    all_gather x1, waiting for transfers between devices, shards(): lax.all_gather(v_ret, 'sp', axis=0, tiled=True)  72.8 us
    all_gather x1, waiting for transfers between devices, shards(): lax.all_gather(v_att, 'sp', axis=0, tiled=True)  72.2 us
    all_gather x1, waiting for transfers between devices, shards(): lax.all_gather(q_ret, 'sp', axis=0, tiled=True)  70.6 us
    all_gather x1, waiting for transfers between devices, all_parts(): parts = lax.all_gather(value, axis, axis=0, tiled=False)  69.9 us
  transfers between devices with their start and end apart: 14, of which 12 were waited for; matrix products, arithmetic and copies ran while one was open for 12% of the time, Pallas kernels for 0%

profile of v1, /device:TPU:0, one launch (start us, length us, event | category | flops | bytes accessed | tf_op | source)
XLA Modules:
  0.0 886.7 jit_solution(8374671692666924115)
XLA Ops:
  7.2 2.5 fusion.6
  13.8 1.2 reduce-window.6
  15.6 2.6 psum.7
  18.3 5.2 all-gather.16.cloned.1.call-done
  23.4 79.6 %all-gather.30.cloned.1.call-done = bf16[4096,512]{1,0:T(8,128)(2,1)} async-done(((bf16[256,512]{1,0:T(8,128)(2,1)}), bf16[4096,512]{1,0:T(8,128)(2,1)}) %all-gather.30.cloned.1.call-update) | async-done | bytes 4194320 | tf_op jit(solution)/shard_map/all_gather | solution.py:93
  103.0 4.1 fusion.17
  107.2 72.8 %all-gather.26.cloned.1.call-done = bf16[4096,512]{1,0:T(8,128)(2,1)} async-done(((bf16[256,512]{1,0:T(8,128)(2,1)}), bf16[4096,512]{1,0:T(8,128)(2,1)}) %all-gather.26.cloned.1.call-update) | async-done | bytes 4194320 | tf_op jit(solution)/shard_map/all_gather | solution.py:94
  180.0 3.5 fusion.19
  183.5 1.1 convolution_convert_fusion
  184.7 1.0 convolution_convert_fusion.1
  188.8 39.8 %all-reduce = bf16[64]{0:T(256)(128)(2,1)S(1)} all-reduce(bf16[64]{0:T(256)(128)(2,1)S(1)} %dynamic-update-slice), channel_id=2, replica_groups=mesh['sp'=16,'tp'=2] {'sp'}, use_global_device_ids=true, to_apply=%add | all-reduce | flops 64 | bytes 256
  230.2 26.9 %all-gather.18.cloned.1.call-done = bf16[4096,512]{1,0:T(8,128)(2,1)} async-done(((bf16[256,512]{1,0:T(8,128)(2,1)}), bf16[4096,512]{1,0:T(8,128)(2,1)}) %all-gather.18.cloned.1.call-update) | async-done | bytes 4194320 | tf_op jit(solution)/shard_map/all_gather | solution.py:90
  257.1 4.1 convolution_multiply_fusion.6
  261.7 72.2 %all-gather.20.cloned.1.call-done = bf16[4096,512]{1,0:T(8,128)(2,1)} async-done(((bf16[256,512]{1,0:T(8,128)(2,1)}), bf16[4096,512]{1,0:T(8,128)(2,1)}) %all-gather.20.cloned.1.call-update) | async-done | bytes 4194320 | tf_op jit(solution)/shard_map/all_gather | solution.py:91
  333.9 4.1 fusion.14
  338.5 3.4 collective-permute-start
  341.8 1.3 collective-permute-start.1
  343.1 69.9 %all-gather.36.cloned.1.call-done = bf16[8192,256]{1,0:T(8,128)(2,1)} async-done(((bf16[512,256]{1,0:T(8,128)(2,1)}), bf16[8192,256]{1,0:T(8,128)(2,1)}) %all-gather.36.cloned.1.call-update) | async-done | bytes 4194320 | tf_op jit(solution)/shard_map/all_gather | solution.py:12
  413.0 6.4 copy.91
  419.4 70.6 %all-gather.28.cloned.1.call-done = bf16[4096,512]{1,0:T(8,128)(2,1)} async-done(((bf16[256,512]{1,0:T(8,128)(2,1)}), bf16[4096,512]{1,0:T(8,128)(2,1)}) %all-gather.28.cloned.1.call-update) | async-done | bytes 4194320 | tf_op jit(solution)/shard_map/all_gather | solution.py:92
  490.0 4.1 fusion.18
  494.1 1.3 convolution_multiply_fusion
  495.6 56.2 %all-gather.34.cloned.1.call-done = bf16[64,128,128]{2,1,0:T(8,128)(2,1)} async-done(((bf16[4,128,128]{2,1,0:T(8,128)(2,1)}), bf16[64,128,128]{2,1,0:T(8,128)(2,1)}) %all-gather.34.cloned.1.call-update) | async-done | bytes 2097168 | tf_op jit(solution)/shard_map/all_gather | solution.py:33
  551.8 27.7 %while.36 = (s32[]{:T(128)}, f32[4,128,128]{2,1,0:T(8,128)S(1)}, s32[]{:T(128)}, bf16[16,4]{1,0:T(8,128)(2,1)}, bf16[16,4,128,128]{3,2,1,0:T(8,128)(2,1)}, /*index=5*/s32[]{:T(128)}, s32[]{:T(128)}, s32[]{:T(128)}, s32[]{:T(128)}) while((s32[]{:T(128)}, f32[4,128,128]{2,1,0:T(8,128)S(1)}, s32[]{:T(128)}, bf16[16,4]{1,0:T(8,128)(2,1)}, ...), condition=%wide.region_9.10_spmd.clone, body=%wide.region_8.9_spmd.clone.sunk | while | flops 327692 | bytes 655567 | solution.py:51
  554.3 1.0 fusion.75
  556.0 1.0 fusion.75
  557.8 1.0 fusion.75
  559.5 1.0 fusion.75
  561.2 1.0 fusion.75
  562.9 1.0 fusion.75
  564.7 1.0 fusion.75
  566.4 1.0 fusion.75
  579.5 1.4 fusion.13
  580.9 32.9 %all-gather.32.cloned.1.call-done = bf16[64,128,128]{2,1,0:T(8,128)(2,1)} async-done(((bf16[4,128,128]{2,1,0:T(8,128)(2,1)}), bf16[64,128,128]{2,1,0:T(8,128)(2,1)}) %all-gather.32.cloned.1.call-update) | async-done | bytes 2097168 | tf_op jit(solution)/shard_map/all_gather | solution.py:33
  613.8 27.7 %while.35 = (s32[]{:T(128)}, f32[4,128,128]{2,1,0:T(8,128)S(1)}, s32[]{:T(128)}, bf16[16,4]{1,0:T(8,128)(2,1)}, bf16[16,4,128,128]{3,2,1,0:T(8,128)(2,1)}, /*index=5*/s32[]{:T(128)}, s32[]{:T(128)}) while((s32[]{:T(128)}, f32[4,128,128]{2,1,0:T(8,128)S(1)}, s32[]{:T(128)}, bf16[16,4]{1,0:T(8,128)(2,1)}, ...), condition=%wide.region_7.8_spmd.clone, body=%wide.region_6.7_spmd.clone.sunk | while | flops 327688 | bytes 655505 | solution.py:51
  623.1 1.0 fusion.74
  624.8 1.0 fusion.74
  633.4 1.0 fusion.74
  641.5 1.4 fusion.12
  642.9 1.7 fusion.50
  644.7 82.9 %all-gather.22.cloned.1.call-done = bf16[4096,1024]{1,0:T(8,128)(2,1)} async-done(((bf16[256,1024]{1,0:T(8,128)(2,1)}), bf16[4096,1024]{1,0:T(8,128)(2,1)}) %all-gather.22.cloned.1.call-update) | async-done | bytes 8388624 | tf_op jit(solution)/shard_map/all_gather | solution.py:89
  727.6 6.3 fusion.8
  734.8 1.0 fusion.4
  736.9 1.3 fusion.9
  738.1 124.8 %all-gather.24.cloned.1.call-done = bf16[1024,4096]{1,0:T(8,128)(2,1)} async-done(((bf16[1024,256]{1,0:T(8,128)(2,1)}), bf16[1024,4096]{1,0:T(8,128)(2,1)}) %all-gather.24.cloned.1.call-update) | async-done | bytes 8388624 | tf_op jit(solution)/shard_map/all_gather | solution.py:188
  863.0 6.0 fusion.51
  869.1 2.7 fusion.2
  872.5 7.4 reduce-scatter.2.cloned.1.call-done
  (153 shorter events, 55.9 us)
Async XLA Ops:
  7.2 6.6 copy-start.4
  7.2 16.3 %all-gather.16.cloned.1.call-start = ((), (), s32[]{:S(2)}) async-start(), calls=%async_computation.1 | async-start | bytes 3145728 | tf_op jit(solution)/shard_map/all_gather | solution.py:98
  9.7 93.3 %all-gather.30.cloned.1.call-start = ((), (), s32[]{:S(2)}) async-start(), calls=%async_computation.8 | async-start | bytes 4456448 | tf_op jit(solution)/shard_map/all_gather | solution.py:93
  10.5 169.5 %all-gather.26.cloned.1.call-start = ((), (), s32[]{:S(2)}) async-start(), calls=%async_computation.6 | async-start | bytes 4456448 | tf_op jit(solution)/shard_map/all_gather | solution.py:94
  11.2 245.8 %all-gather.18.cloned.1.call-start = ((), (), s32[]{:S(2)}) async-start(), calls=%async_computation.2 | async-start | bytes 4456448 | tf_op jit(solution)/shard_map/all_gather | solution.py:90
  11.8 322.1 %all-gather.20.cloned.1.call-start = ((), (), s32[]{:S(2)}) async-start(), calls=%async_computation.3 | async-start | bytes 4456448 | tf_op jit(solution)/shard_map/all_gather | solution.py:91
  12.4 400.6 %all-gather.36.cloned.1.call-start = ((), (), s32[]{:S(2)}) async-start(), calls=%async_computation.12 | async-start | bytes 4456448 | tf_op jit(solution)/shard_map/all_gather | solution.py:12
  13.0 477.0 %all-gather.28.cloned.1.call-start = ((), (), s32[]{:S(2)}) async-start(), calls=%async_computation.7 | async-start | bytes 4456448 | tf_op jit(solution)/shard_map/all_gather | solution.py:92
  13.7 538.1 %all-gather.34.cloned.1.call-start = ((), (), s32[]{:S(2)}) async-start(), calls=%async_computation.11 | async-start | bytes 2228224 | tf_op jit(solution)/shard_map/all_gather | solution.py:33
  18.2 315.7 %copy-start.7 = (f32[256]{0:T(256)}, f32[256]{0:T(256)S(1)}, u32[]{:S(2)}) copy-start(f32[256]{0:T(256)S(1)} %get-tuple-element.322) | copy-start | bytes 3076
  23.4 156.6 %copy-start.10 = (bf16[256,4096]{1,0:T(8,128)(2,1)S(1)}, bf16[256,4096]{1,0:T(8,128)(2,1)}, u32[]{:S(2)}) copy-start(bf16[256,4096]{1,0:T(8,128)(2,1)} %all-gather.16.cloned.1.call-done) | copy-start | bytes 6291460
  180.0 7.3 copy-start.11
  180.0 49.3 %copy-start.5 = (f32[8]{0:T(128)S(1)}, f32[8]{0:T(128)}, u32[]{:S(2)}) copy-start(f32[8]{0:T(128)} %param.26) | copy-start | bytes 100
  183.5 3.6 copy-start.3
  184.6 429.1 %all-gather.32.cloned.1.call-start = ((), (), s32[]{:S(2)}) async-start(), calls=%async_computation.10 | async-start | bytes 2228224 | tf_op jit(solution)/shard_map/all_gather | solution.py:33
  185.8 541.8 %all-gather.22.cloned.1.call-start = ((), (), s32[]{:S(2)}) async-start(), calls=%async_computation.4 | async-start | bytes 8912896 | tf_op jit(solution)/shard_map/all_gather | solution.py:89
  186.4 676.6 %all-gather.24.cloned.1.call-start = ((), (), s32[]{:S(2)}) async-start(), calls=%async_computation.5 | async-start | bytes 8912896 | tf_op jit(solution)/shard_map/all_gather | solution.py:188
  187.1 692.8 %reduce-scatter.2.cloned.1.call-start = ((), (), s32[]{:S(2)}) async-start(), calls=%async_computation.9 | async-start | bytes 3145728 | tf_op jit(solution)/shard_map/reduce_scatter | solution.py:191
  338.5 156.9 %collective-permute-start = (bf16[2,128,4,128]{3,1,2,0:T(8,128)(2,1)S(1)}, bf16[2,128,4,128]{3,1,2,0:T(8,128)(2,1)S(1)}, u32[]{:S(2)}, u32[]{:S(2)}) collective-permute-start(bf16[2,128,4,128]{3,1,2,0:T(8,128)(2,1)S(1)} %get-tuple-element.313), channel_id=1, source_target_pairs={{0,2},{2,4},{4,6},{6,8},{8,10},{10,12},{12,14},{14,16},{16,18},{18... | collective-permute-start | bytes 786440 | tf_op jit(solution)/shard_map/ppermute | solution.py:24
  341.8 153.6 %collective-permute-start.1 = (bf16[2,128,4,128]{3,1,2,0:T(8,128)(2,1)S(1)}, bf16[2,128,4,128]{3,1,2,0:T(8,128)(2,1)S(1)}, u32[]{:S(2)}, u32[]{:S(2)}) collective-permute-start(bf16[2,128,4,128]{3,1,2,0:T(8,128)(2,1)S(1)} %get-tuple-element.314), channel_id=1, source_target_pairs={{2,0},{4,2},{6,4},{8,6},{10,8},{12,10},{14,12},{16,14},{18,16},{20... | collective-permute-start | bytes 786440 | tf_op jit(solution)/shard_map/ppermute | solution.py:25
  413.0 77.0 %copy-start.8 = (f32[256]{0:T(256)S(1)}, f32[256]{0:T(256)}, u32[]{:S(2)}) copy-start(f32[256]{0:T(256)} %copy-done.7) | copy-start | bytes 3076
  494.1 1.3 copy-start.2
  551.8 91.1 %copy-start.1 = (f32[4,256,256]{2,1,0:T(8,128)S(1)}, f32[4,256,256]{2,1,0:T(8,128)}, u32[]{:S(2)}) copy-start(f32[4,256,256]{2,1,0:T(8,128)} %convolution_multiply_fusion) | copy-start | bytes 3145732
  613.8 113.8 %copy-start.9 = (f32[256]{0:T(256)S(1)}, f32[256]{0:T(256)}, u32[]{:S(2)}) copy-start(f32[256]{0:T(256)} %copy-done.7) | copy-start | bytes 3076
  863.0 6.1 copy-start
  869.1 2.8 copy-start.6
Sparse Core Ops, SparseCore 0:
  10.1 13.2 all-gather.15
  26.2 76.7 all-gather.29
  105.8 74.1 all-gather.25
  182.6 74.3 all-gather.17
  259.7 74.1 all-gather.19
  336.5 76.4 all-gather.35
  415.8 74.1 all-gather.27
  492.8 58.9 all-gather.33
  554.6 59.1 all-gather.31
  616.4 111.1 all-gather.21
  730.3 132.6 all-gather.23
  871.9 7.9 reduce-scatter.1
